TPU v7x, 32 devices: a whole 2x2x4 slice. The times are simulated.
32 devices in a mesh: ep: 32 (over z, y, x, core).
Axes of the slice: x: 2, y: 2, z: 4, core: 2. Of those that a mesh axis runs over, the one named last changes fastest.
Arguments:
- tokens: bfloat16 [128, 2048], P('ep'), may hold values from -6 to 6
- recurrent_state: float32 [128, 8, 128, 128], P('ep'), may hold values from -4 to 4
- query_weight: bfloat16 [2048, 1024], P(None, 'ep'), may hold values from -0.125 to 0.125
- forget_weight: bfloat16 [2048, 1024], P(None, 'ep'), may hold values from -0.125 to 0.125
- input_weight: bfloat16 [2048, 1024], P(None, 'ep'), may hold values from -0.125 to 0.125
- outgate_weight: bfloat16 [2048, 1024], P(None, 'ep'), may hold values from -0.125 to 0.125
- lower_bound: float32 [1024], replicated, may hold values from 0 to 0.9
- head_gain: float32 [128], replicated, may hold values from 0.1 to 1.9
- mixout_weight: bfloat16 [1024, 2048], P(None, 'ep'), may hold values from -0.1875 to 0.1875
- first_gain: float32 [2048], replicated, may hold values from 0.1 to 1.9
- first_bias: float32 [2048], replicated, may hold values from -1.5 to 1.5
- router_weight: bfloat16 [2048, 8], replicated, may hold values from -0.125 to 0.125
- branch_vector: bfloat16 [2048], replicated, may hold values from -0.125 to 0.125
- dense_gate_weight: bfloat16 [2048, 5632], P(None, 'ep'), may hold values from -0.125 to 0.125
- dense_up_weight: bfloat16 [2048, 5632], P(None, 'ep'), may hold values from -0.125 to 0.125
- dense_down_weight: bfloat16 [5632, 2048], P('ep'), may hold values from -0.078125 to 0.078125
- expert_gate_weight: bfloat16 [2048, 57344], P(None, 'ep'), may hold values from -0.125 to 0.125
- expert_up_weight: bfloat16 [2048, 57344], P(None, 'ep'), may hold values from -0.125 to 0.125
- expert_down_weight: bfloat16 [57344, 2048], P('ep'), may hold values from -0.0625 to 0.0625
- second_gain: float32 [2048], replicated, may hold values from 0.1 to 1.9
- second_bias: float32 [2048], replicated, may hold values from -1.5 to 1.5
- routes: int32 [128, 2], replicated, may hold values from 0 to 7, all different within a row; in each aligned block of 4 rows (0 to 3, 4 to 7, ...) at most 2 rows name the same one
Outputs:
- output: bfloat16 [128, 2048], P('ep')
- new_state: float32 [128, 8, 128, 128], P('ep')
Inputs may be any that keep to these rules, and one draw needn't show every extreme that they name: `routes`: each row names two different experts; in the rows of one device no expert is named more than 2 times, a bound that some block reaches in some device's rows.
All inputs are finite; a program needn't handle non-finite values.
Results may differ from a plain program's by a relative error of at most 0.0095.
Values may be sent and summed in bfloat16 or wider, within the bound.
A program may use at most 64 MiB of HBM per device.

v0:
```python
import jax
import jax.numpy as jnp
from jax import lax
import functools

from jax.experimental import pallas as pl
from jax.experimental.pallas import tpu as pltpu
from jax.sharding import PartitionSpec as P

EXPERTS = 8
MESH = pl.DeviceIdType.MESH


ALPHA = 8.0**0.25
NORM_EPS = 1e-05
HEAD_EPS = 1e-06


def layer_norm(mixture, gain, bias):
    center = jnp.mean(mixture, axis=-1, keepdims=True)
    spread = jnp.mean(jnp.square(mixture - center), axis=-1, keepdims=True)
    return (mixture - center) * lax.rsqrt(spread + NORM_EPS) * gain + bias


def recurrence(projected, state, lower_bound, head_gain):
    nseq, heads, width = (state.shape[0], state.shape[1], state.shape[2])
    query = projected[:, 0].astype(jnp.float32).reshape(nseq, heads, width)
    forget_in = projected[:, 1].astype(jnp.float32)
    value = projected[:, 2].astype(jnp.float32).reshape(nseq, heads, width)
    outgate = projected[:, 3].astype(jnp.float32)
    forget = (lower_bound + (1.0 - lower_bound) * jax.nn.sigmoid(forget_in)).reshape(
        nseq, heads, width
    )
    keyed = ((1.0 - lower_bound) * jax.nn.sigmoid(-forget_in)).reshape(nseq, heads, width)
    fresh = forget[..., None] * state + keyed[..., None] * value[:, :, None, :]
    read = jnp.einsum("bhkv,bhk->bhv", fresh, query, precision=lax.Precision.HIGHEST)
    scaled = (
        read * lax.rsqrt(jnp.mean(jnp.square(read), axis=-1, keepdims=True) + HEAD_EPS) * head_gain
    )
    mixed = (scaled.reshape(nseq, heads * width) * jax.nn.silu(outgate)).astype(jnp.bfloat16)
    return (mixed, fresh)


def greet(n, me):
    barrier = pltpu.get_barrier_semaphore()

    @pl.loop(1, n)
    def _(k):
        pl.semaphore_signal(
            barrier, inc=1, device_id=(lax.rem(me + k, n),), device_id_type=MESH
        )

    pl.semaphore_wait(barrier, n - 1)


def start_all(source, dest, send_sem, recv_sem, n, me):
    @pl.loop(1, n)
    def _(k):
        peer = lax.rem(me + k, n)
        pltpu.make_async_remote_copy(
            src_ref=source(peer),
            dst_ref=dest.at[me],
            send_sem=send_sem.at[k],
            recv_sem=recv_sem.at[k],
            device_id=(peer,),
            device_id_type=MESH,
        ).start()


def wait_all(source, dest, send_sem, recv_sem, n, me):
    @pl.loop(1, n)
    def _(k):
        peer = lax.rem(me + k, n)
        pltpu.make_async_remote_copy(
            src_ref=source(peer),
            dst_ref=dest.at[lax.rem(me + n - k, n)],
            send_sem=send_sem.at[k],
            recv_sem=recv_sem.at[k],
            device_id=(peer,),
            device_id_type=MESH,
        ).wait()


def gather_all(block_ref, gathered, send_sem, recv_sem, n, me):
    chips = n // 2
    chip, core = lax.div(me, 2), lax.rem(me, 2)
    sibling = 2 * chip + 1 - core

    def across(k, owner):
        return pltpu.make_async_remote_copy(
            src_ref=block_ref,
            dst_ref=gathered.at[owner],
            send_sem=send_sem.at[k],
            recv_sem=recv_sem.at[k],
            device_id=(2 * lax.rem(chip + k, chips) + core,),
            device_id_type=MESH,
        )

    def onward(k, source, owner):
        return pltpu.make_async_remote_copy(
            src_ref=source,
            dst_ref=gathered.at[owner],
            send_sem=send_sem.at[chips + k],
            recv_sem=recv_sem.at[chips + k],
            device_id=(sibling,),
            device_id_type=MESH,
        )

    pl.loop(1, chips)(lambda k: across(k, me).start())
    onward(0, block_ref, me).start()
    gathered[me] = block_ref[...]

    @pl.loop(1, chips)
    def _(k):
        owner = 2 * lax.rem(chip + chips - k, chips) + core
        across(k, owner).wait()
        onward(k, gathered.at[owner], owner).start()

    onward(0, block_ref, sibling).wait()

    @pl.loop(1, chips)
    def _(k):
        base = 2 * lax.rem(chip + chips - k, chips)
        onward(k, gathered.at[base + core], base + 1 - core).wait()


def dot_turned(rows, weight):
    return lax.dot_general(
        rows, weight, (((1,), (1,)), ((), ())), preferred_element_type=jnp.float32
    )


def flatten_rows(blocks, flat, n, nseq):
    group = max(1, 16 // nseq)

    @pl.loop(0, n // group)
    def _(i):
        parts = [blocks[i * group + j].astype(jnp.float32) for j in range(group)]
        at = pl.multiple_of(i * (group * nseq), group * nseq)
        flat[pl.ds(at, group * nseq), :] = jnp.concatenate(parts, axis=0).astype(flat.dtype)


def split_rows(flat, blocks, n, nseq):
    group = max(1, 8 // nseq)

    @pl.loop(0, n // group)
    def _(i):
        at = pl.multiple_of(i * (group * nseq), group * nseq)
        taken = flat[pl.ds(at, group * nseq), :]
        for j in range(group):
            blocks[i * group + j] = taken[j * nseq : (j + 1) * nseq].astype(blocks.dtype)


def project_kernel(
    n, block_ref, weight_hbm, out_ref,
    weight, gathered, rows, made, outgoing, landed,
    weight_sem, gather_send, gather_recv, back_send, back_recv,
):
    me = lax.axis_index("ep")
    nseq = block_ref.shape[0]
    load = pltpu.make_async_copy(weight_hbm, weight, weight_sem)
    load.start()
    greet(n, me)
    gather_all(block_ref, gathered, gather_send, gather_recv, n, me)
    flatten_rows(gathered, rows, n, nseq)
    load.wait()
    made[...] = dot_turned(rows[...], weight[...])
    split_rows(made, outgoing, n, nseq)
    part = lambda peer: outgoing.at[peer]
    start_all(part, landed, back_send, back_recv, n, me)
    landed[me] = outgoing[me]
    wait_all(part, landed, back_send, back_recv, n, me)
    out_ref[...] = landed[...]


def exchange_semaphores(n):
    return [pltpu.SemaphoreType.DMA((n,))] * 4


def project(block, weight, n, collective_id):
    nseq, width = block.shape
    cols = weight.shape[0]
    bf16, f32 = jnp.bfloat16, jnp.float32
    return pl.pallas_call(
        functools.partial(project_kernel, n),
        out_shape=jax.ShapeDtypeStruct((n, nseq, cols), bf16),
        in_specs=[
            pl.BlockSpec(memory_space=pltpu.VMEM),
            pl.BlockSpec(memory_space=pl.ANY),
        ],
        out_specs=pl.BlockSpec(memory_space=pltpu.VMEM),
        scratch_shapes=[
            pltpu.VMEM(weight.shape, bf16),
            pltpu.VMEM((n, nseq, width), bf16),
            pltpu.VMEM((n * nseq, width), bf16),
            pltpu.VMEM((n * nseq, cols), f32),
            pltpu.VMEM((n, nseq, cols), bf16),
            pltpu.VMEM((n, nseq, cols), bf16),
            pltpu.SemaphoreType.DMA,
            *exchange_semaphores(n),
        ],
        compiler_params=pltpu.CompilerParams(
            collective_id=collective_id, has_side_effects=True, vmem_limit_bytes=24 * 2**20
        ),
    )(block, weight)


def column_tile(cols):
    return 256 if cols % 256 == 0 else cols


def for_tiles(cols, body):
    tile = column_tile(cols)
    if tile == cols:
        body(slice(None))
    else:
        pl.loop(0, cols // tile)(lambda i: body(pl.ds(pl.multiple_of(i * tile, tile), tile)))


def channel_kernel(
    n, block_ref, pick_ref, small_ref, gain_ref, bias_ref,
    gate_hbm, up_hbm, down_hbm, dense_gate_hbm, dense_up_hbm, dense_down_hbm, out_ref,
    gate_w, up_w, down_w, dense_gate_w, dense_up_w, dense_down_w,
    gathered, rows, hidden, dense_hidden, made, outgoing, landed,
    weight_sem, gather_send, gather_recv, back_send, back_recv,
):
    f32 = jnp.float32
    me = lax.axis_index("ep")
    nseq, width = block_ref.shape
    pairs = (
        (dense_gate_hbm, dense_gate_w),
        (dense_up_hbm, dense_up_w),
        (gate_hbm, gate_w),
        (up_hbm, up_w),
        (dense_down_hbm, dense_down_w),
        (down_hbm, down_w),
    )
    loads = [
        pltpu.make_async_copy(there, here, weight_sem.at[i]) for i, (there, here) in enumerate(pairs)
    ]
    for load in loads:
        load.start()
    greet(n, me)
    gather_all(block_ref, gathered, gather_send, gather_recv, n, me)
    flatten_rows(gathered, rows, n, nseq)
    dot = functools.partial(jnp.dot, preferred_element_type=f32)

    small = dot_turned(rows[...], small_ref[...])
    picks = pick_ref[...]
    logit_gap = jnp.sum(small[:, :EXPERTS] * picks[:, :EXPERTS], axis=1, keepdims=True)
    share = jax.nn.sigmoid(logit_gap)
    branch_gate = jax.nn.sigmoid(small[:, EXPERTS : EXPERTS + 1])
    on_first = picks[:, EXPERTS : EXPERTS + 1] > 0
    on_second = picks[:, EXPERTS + 1 : EXPERTS + 2] > 0
    weight = jnp.where(on_first, share, jnp.where(on_second, 1.0 - share, 0.0))

    def fill(target, gate, up):
        def body(at):
            gate_part = dot(rows[...], gate[:, at])
            up_part = dot(rows[...], up[:, at])
            target[:, at] = (jax.nn.silu(gate_part) * up_part).astype(jnp.bfloat16)

        for_tiles(target.shape[1], body)

    for load in loads[:2]:
        load.wait()
    gate_part = dot_turned(rows[...], dense_gate_w[...])
    up_part = dot_turned(rows[...], dense_up_w[...])
    dense_hidden[...] = (jax.nn.silu(gate_part) * up_part).astype(jnp.bfloat16)
    for load in loads[2:4]:
        load.wait()
    fill(hidden, gate_w, up_w)
    for load in loads[4:]:
        load.wait()

    def down(at):
        routed = dot(hidden[...], down_w[:, at])
        dense = dot(dense_hidden[...], dense_down_w[:, at])
        made[:, at] = branch_gate * dense + jnp.where(weight > 0, weight * routed, 0.0)

    for_tiles(width, down)
    split_rows(made, outgoing, n, nseq)
    part = lambda peer: outgoing.at[peer]
    start_all(part, landed, back_send, back_recv, n, me)
    landed[me] = outgoing[me]
    wait_all(part, landed, back_send, back_recv, n, me)
    channel = lax.fori_loop(
        0, n, lambda d, total: total + landed[d].astype(f32), jnp.zeros((nseq, width), f32)
    )
    mixture = ALPHA * block_ref[...].astype(f32) + channel
    out_ref[...] = layer_norm(mixture, gain_ref[...], bias_ref[...]).astype(jnp.bfloat16)


def channel_and_norm(
    normed, routes, n, router_weight, branch_vector, dense_gate_weight, dense_up_weight,
    dense_down_weight, expert_gate_weight, expert_up_weight, expert_down_weight, gain, bias,
):
    bf16, f32 = jnp.bfloat16, jnp.float32
    nseq, width = normed.shape
    total = n * nseq
    expert = lax.axis_index("ep") // (n // EXPERTS)
    first = jax.nn.one_hot(routes[:, 0], EXPERTS, dtype=f32)
    second = jax.nn.one_hot(routes[:, 1], EXPERTS, dtype=f32)
    picks = jnp.concatenate([first - second, (routes == expert).astype(f32)], axis=1)
    small = jnp.concatenate([router_weight.T, branch_vector[None]], axis=0)
    weights = (
        expert_gate_weight,
        expert_up_weight,
        expert_down_weight,
        dense_gate_weight.T,
        dense_up_weight.T,
        dense_down_weight,
    )
    vmem, anywhere = pl.BlockSpec(memory_space=pltpu.VMEM), pl.BlockSpec(memory_space=pl.ANY)
    return pl.pallas_call(
        functools.partial(channel_kernel, n),
        out_shape=jax.ShapeDtypeStruct((nseq, width), bf16),
        in_specs=[vmem] * 5 + [anywhere] * 6,
        out_specs=vmem,
        scratch_shapes=[
            *[pltpu.VMEM(w.shape, bf16) for w in weights],
            pltpu.VMEM((n, nseq, width), bf16),
            pltpu.VMEM((total, width), bf16),
            pltpu.VMEM((total, expert_gate_weight.shape[1]), bf16),
            pltpu.VMEM((total, dense_gate_weight.shape[1]), bf16),
            pltpu.VMEM((total, width), f32),
            pltpu.VMEM((n, nseq, width), bf16),
            pltpu.VMEM((n, nseq, width), bf16),
            pltpu.SemaphoreType.DMA((6,)),
            *exchange_semaphores(n),
        ],
        compiler_params=pltpu.CompilerParams(
            collective_id=2, has_side_effects=True, vmem_limit_bytes=56 * 2**20
        ),
    )(normed, picks, small, gain[None], bias[None], *weights)


def per_device(
    tokens,
    recurrent_state,
    query_weight,
    forget_weight,
    input_weight,
    outgate_weight,
    lower_bound,
    head_gain,
    mixout_weight,
    first_gain,
    first_bias,
    router_weight,
    branch_vector,
    dense_gate_weight,
    dense_up_weight,
    dense_down_weight,
    expert_gate_weight,
    expert_up_weight,
    expert_down_weight,
    second_gain,
    second_bias,
    routes,
):
    f32 = jnp.float32
    devices = lax.axis_size("ep")
    nseq, width = tokens.shape
    own_cols = query_weight.shape[1]
    stacked = jnp.concatenate(
        [query_weight.T, forget_weight.T, input_weight.T, outgate_weight.T], axis=0
    )
    owned = project(tokens, stacked, devices, 0)
    projected = (
        owned.reshape(devices, nseq, 4, own_cols)
        .transpose(1, 2, 0, 3)
        .reshape(nseq, 4, devices * own_cols)
    )
    mixed, new_state = recurrence(projected, recurrent_state, lower_bound, head_gain)
    mix_out = project(mixed, mixout_weight.T, devices, 1).transpose(1, 0, 2).reshape(nseq, width)
    normed = layer_norm(
        ALPHA * tokens.astype(f32) + mix_out.astype(f32), first_gain, first_bias
    ).astype(jnp.bfloat16)
    output = channel_and_norm(
        normed,
        routes,
        devices,
        router_weight,
        branch_vector,
        dense_gate_weight,
        dense_up_weight,
        dense_down_weight,
        expert_gate_weight,
        expert_up_weight,
        expert_down_weight,
        second_gain,
        second_bias,
    )
    return (output, new_state)


def solution(mesh):
    return jax.shard_map(
        per_device,
        mesh=mesh,
        in_specs=(
            P("ep", None),
            P("ep", None, None, None),
            P(None, "ep"),
            P(None, "ep"),
            P(None, "ep"),
            P(None, "ep"),
            P(),
            P(),
            P(None, "ep"),
            P(),
            P(),
            P(),
            P(),
            P(None, "ep"),
            P(None, "ep"),
            P("ep", None),
            P(None, "ep"),
            P(None, "ep"),
            P("ep", None),
            P(),
            P(),
            P(),
        ),
        out_specs=(P("ep", None), P("ep", None, None, None)),
        check_vma=False,
    )
```

profile of v0, /device:TPU:29, one launch (start us, length us, event | category | flops | bytes accessed | tf_op | source)
XLA Modules:
  0.0 81.7 jit_solution(12608013460540657157)
XLA Ops:
  0.6 0.0 copy-start.5
  0.6 1.1 %pad_maximum_fusion.weight_hbm = bf16[128,2048]{1,0:T(8,128)(2,1)S(1)} fusion(bf16[32,2048]{1,0:T(8,128)(2,1)} %bitcast.70, bf16[32,2048]{1,0:T(8,128)(2,1)} %bitcast.71, bf16[32,2048]{1,0:T(8,128)(2,1)} %bitcast.72, bf16[32,2048]{1,0:T(8,128)(2,1)} %bitcast.73), kind=kLoop, calls=%fused_computation.1 | loop fusion | flops 2097152 | bytes 1048576 | tf_op jit(solution)/shard_map/concatenate | solution.py:366
  1.8 0.0 copy-start
  1.8 0.7 copy-done
  2.5 17.8 %shard_map.221 = bf16[32,4,128]{2,1,0:T(4,128)(2,1)S(1)} custom-call(bf16[4,2048]{1,0:T(4,128)(2,1)S(1)} %copy-done, bf16[128,2048]{1,0:T(8,128)(2,1)S(1)} %pad_maximum_fusion.weight_hbm), custom_call_target="tpu_custom_call" | custom-call | tf_op jit(solution)/shard_map/pallas_call | solution.py:184
  20.3 0.1 reshape.102
  20.5 0.2 reshape.103
  20.7 0.0 copy-done.5
  20.8 2.5 %multiply_add_fusion = f32[4,8,128,128]{3,2,1,0:T(8,128)S(1)} fusion(f32[4,8,128,128]{3,2,1,0:T(8,128)} %param.23, f32[4,8,128]{2,1,0:T(8,128)S(1)} %bitcast.74, f32[4,8,128]{2,1,0:T(8,128)S(1)} %get-tuple-element.7, f32[4,8,128]{2,1,0:T(8,128)S(1)} %get-tuple-element.6), kind=kLoop, calls=%fused_computation | loop fusion | flops 1572864 | bytes 4243456 | tf_op jit(solution)/shard_map/add | solution.py:35
  23.2 0.0 copy-start.3
  23.3 0.0 copy-start.10
  23.3 0.0 copy-start.2
  23.3 0.0 copy-start.1
  23.3 0.0 copy-start.6
  23.3 0.0 copy-start.7
  23.3 0.0 copy-start.9
  23.3 0.0 copy-start.8
  23.3 0.0 copy-start.4
  23.4 1.1 %fusion.14 = f32[4,8,1,128]{3,2,1,0:T(1,128)S(1)} fusion(f32[4,8,128,128]{3,2,1,0:T(8,128)S(1)} %multiply_add_fusion, bf16[4,8,128,1]{2,3,1,0:T(2,128)(2,1)S(1)} %reshape.114), kind=kOutput, calls=%fused_computation.44 | convolution fusion | flops 6291456 | bytes 2121728 | tf_op jit(solution)/shard_map/bhkv,bhk->bhv/dot_general | solution.py:36
  24.4 0.1 multiply_reduce_fusion.1
  24.5 0.0 copy-done.10
  24.5 0.1 multiply_bitcast_fusion
  24.6 0.0 copy-done.2
  24.7 16.6 %shard_map.222 = bf16[32,4,64]{2,1,0:T(4,128)(2,1)S(1)} custom-call(bf16[4,1024]{1,0:T(4,128)(2,1)S(1)} %fusion.11.block_ref, bf16[64,1024]{1,0:T(8,128)(2,1)S(1)} %bitcast.64), custom_call_target="tpu_custom_call" | custom-call | tf_op jit(solution)/shard_map/pallas_call | solution.py:184
  41.3 0.1 reshape.110
  41.4 0.0 copy-done.1
  41.4 0.1 fusion.12
  41.5 0.2 multiply_reduce_fusion
  41.7 0.0 copy-done.6
  41.7 0.0 copy-done.7
  41.7 0.7 add_convert_fusion.block_ref
  42.4 0.0 copy-done.9
  42.5 0.7 copy.30.pick_ref
  43.2 0.0 copy-done.8
  43.2 0.0 copy-done.4
  43.2 0.6 pad_maximum_fusion.1.small_ref
  43.9 36.5 %shard_map.223 = bf16[4,2048]{1,0:T(4,128)(2,1)} custom-call(bf16[4,2048]{1,0:T(4,128)(2,1)} %add_convert_fusion.block_ref, f32[128,10]{1,0:T(8,128)} %copy.30.pick_ref, bf16[9,2048]{1,0:T(8,128)(2,1)} %pad_maximum_fusion.1.small_ref, f32[1,2048]{1,0:T(1,128)} %bitcast.77, f32[1,2048]{1,0:T(1,128)} %bitcast.78, bf16[2048,1792]{1,0:T(8,128)(2,1)} %gate_hbm.1, ...), custom_call_target="tpu_custom_call" | custom-call | tf_op jit(solution)/shard_map/pallas_call | solution.py:315
  80.3 0.0 copy-done.3
  80.4 1.3 %copy.47 = bf16[4,2048]{1,0:T(4,128)(2,1)} copy(bf16[4,2048]{1,0:T(4,128)(2,1)} %shard_map.223) | data formatting | bytes 32768
  (18 shorter events, 0.2 us)
Async XLA Ops:
  0.6 20.1 %copy-start.5 = (f32[1024]{0:T(1024)S(1)}, f32[1024]{0:T(1024)}, u32[]{:S(2)}) copy-start(f32[1024]{0:T(1024)} %param.28) | copy-start | bytes 12292
  1.8 0.7 copy-start
  23.2 57.1 %copy-start.3 = (f32[4,8,128,128]{3,2,1,0:T(8,128)}, f32[4,8,128,128]{3,2,1,0:T(8,128)S(1)}, u32[]{:S(2)}) copy-start(f32[4,8,128,128]{3,2,1,0:T(8,128)S(1)} %multiply_add_fusion) | copy-start | bytes 6291460
  23.3 1.3 %copy-start.10 = (f32[128]{0:T(128)S(1)}, f32[128]{0:T(128)}, u32[]{:S(2)}) copy-start(f32[128]{0:T(128)} %param.29) | copy-start | bytes 1540
  23.3 1.4 %copy-start.2 = (bf16[1024,64]{0,1:T(8,128)(2,1)S(1)}, bf16[1024,64]{0,1:T(8,128)(2,1)}, u32[]{:S(2)}) copy-start(bf16[1024,64]{0,1:T(8,128)(2,1)} %param.30) | copy-start | bytes 393220
  23.3 18.1 %copy-start.1 = (bf16[4,2048]{1,0:T(4,128)(2,1)S(1)}, bf16[4,2048]{1,0:T(4,128)(2,1)}, u32[]{:S(2)}) copy-start(bf16[4,2048]{1,0:T(4,128)(2,1)} %block_ref.1) | copy-start | bytes 49156
  23.3 18.4 %copy-start.6 = (f32[2048]{0:T(1024)S(1)}, f32[2048]{0:T(1024)}, u32[]{:S(2)}) copy-start(f32[2048]{0:T(1024)} %param.32) | copy-start | bytes 24580
  23.3 18.4 %copy-start.7 = (f32[2048]{0:T(1024)S(1)}, f32[2048]{0:T(1024)}, u32[]{:S(2)}) copy-start(f32[2048]{0:T(1024)} %param.31) | copy-start | bytes 24580
  23.3 19.1 %copy-start.9 = (s32[128,2]{0,1:T(2,128)S(1)}, s32[128,2]{0,1:T(2,128)}, u32[]{:S(2)}) copy-start(s32[128,2]{0,1:T(2,128)} %param.43) | copy-start | bytes 3076
  23.3 19.9 %copy-start.8 = (bf16[2048]{0:T(1024)(128)(2,1)S(1)}, bf16[2048]{0:T(1024)(128)(2,1)}, u32[]{:S(2)}) copy-start(bf16[2048]{0:T(1024)(128)(2,1)} %param.34) | copy-start | bytes 12292
  23.3 19.9 %copy-start.4 = (bf16[2048,8]{0,1:T(8,128)(2,1)S(1)}, bf16[2048,8]{0,1:T(8,128)(2,1)}, u32[]{:S(2)}) copy-start(bf16[2048,8]{0,1:T(8,128)(2,1)} %param.33) | copy-start | bytes 98308
where the time goes:
time: 82 us; the launch traced here: 81.7 us
  Pallas kernels  70.8 us (86%)
  other arithmetic  5.57 us (7%)
  local copies, waits for them, and re-layouts  3.29 us (4%)
  matrix products  1.06 us (1%)
  between operations  0.92 us (1%)
    pallas_call x1, Pallas kernels, channel_and_norm(): pl.pallas_call(functools.partial(channel_kernel, n), out_shape=jax.ShapeD...  36.5 us
    pallas_call x2, Pallas kernels, project(): pl.pallas_call(functools.partial(project_kernel, n), out_shape=jax.ShapeD...  34.4 us
    add x1, other arithmetic, recurrence(): fresh = forget[..., None] * state + keyed[..., None] * value[:, :, None, :]  2.48 us
    unnamed x24, local copies, waits for them, and re-layouts  2.11 us

commit v1 on v0

--- a/solution.py
+++ b/solution.py
@@ -8,6 +8,7 @@
 from jax.sharding import PartitionSpec as P
 
 EXPERTS = 8
+CHUNKS = 4
 MESH = pl.DeviceIdType.MESH
 
 
@@ -335,6 +336,395 @@
     )(normed, picks, small, gain[None], bias[None], *weights)
 
 
+def parity_peers(chip, chips):
+    bits = [1 << i for i in range(chips.bit_length() - 1)]
+    steps = [(1 - 2 * lax.rem(lax.div(chip, bit), 2)) * bit for bit in bits]
+    peers = []
+    for k in range(chips):
+        peer = chip
+        for bit, step in zip(bits, steps):
+            if k & bit:
+                peer = peer + step
+        peers.append(peer)
+    return peers
+
+
+def remote(source, dest, send_sem, recv_sem, device):
+    return pltpu.make_async_remote_copy(
+        src_ref=source, dst_ref=dest, send_sem=send_sem, recv_sem=recv_sem,
+        device_id=(device,), device_id_type=MESH,
+    )
+
+
+def stack_rows(blocks, flat, chips, nseq):
+    group = 16 // nseq
+    for i in range(chips // group):
+        parts = [blocks[i * group + j].astype(jnp.float32) for j in range(group)]
+        flat[i * 16 : (i + 1) * 16, :] = jnp.concatenate(parts, axis=0).astype(flat.dtype)
+
+
+def layer_kernel(
+    n, chunks,
+    tokens_hbm, state_hbm, query_hbm, forget_hbm, value_hbm, outgate_hbm, bound_hbm, head_gain_hbm,
+    mixout_hbm, first_gain_hbm, first_bias_hbm, router_hbm, branch_hbm,
+    dense_gate_hbm, dense_up_hbm, dense_down_hbm, gate_hbm, up_hbm, down_hbm,
+    second_gain_hbm, second_bias_hbm, routes_hbm,
+    out_ref, fresh_ref,
+    state, query_w, mix_w, gate_w, up_w, down_w, dense_gate_w, dense_up_w, dense_down_w,
+    bound, head_gain, first_gain, first_bias, router, branch, second_gain, second_bias, routes,
+    tok_blocks, tok_rows, made_out, made_in, mix_blocks, mix_rows, feats, normed,
+    state_high, state_low, small_w, hidden, dense_hidden, own_part, pair_out, pair_in,
+    outgoing, landed,
+    load_sem, a_send, a_recv, b_send, b_recv, c_send, c_recv, d_send, d_recv, f_send, f_recv,
+    pair_send, pair_recv,
+):
+    bf16, f32 = jnp.bfloat16, jnp.float32
+    me = lax.axis_index("ep")
+    chips = n // 2
+    chip, core = lax.div(me, 2), lax.rem(me, 2)
+    sibling = 2 * chip + 1 - core
+    peers = parity_peers(chip, chips)
+    devices = [2 * peer + core for peer in peers]
+    order = list(range(chips - 1, 0, -1))
+    nseq, width = tokens_hbm.shape
+    heads, depth = bound.shape
+    half = chips * nseq
+    own = query_hbm.shape[0]
+    mix_own = mixout_hbm.shape[0]
+    at_core = lambda base, size: pl.ds(pl.multiple_of(base + core * size, size), size)
+
+    loads = []
+
+    def load(there, here):
+        copy = pltpu.make_async_copy(there, here, load_sem.at[len(loads)])
+        copy.start()
+        loads.append(copy)
+        return copy
+
+    get_tokens = load(tokens_hbm, tok_blocks.at[chip])
+    pieces = (query_hbm, forget_hbm, value_hbm, outgate_hbm)
+    spots = [query_w.at[at_core(m * 2 * own, own)] for m in range(4)]
+    get_proj = [load(piece, spot) for piece, spot in zip(pieces, spots)]
+    mix_spot = mix_w.at[at_core(0, mix_own)]
+    get_mix = load(mixout_hbm, mix_spot)
+    get_small = [
+        load(there, here)
+        for there, here in (
+            (bound_hbm, bound), (head_gain_hbm, head_gain), (first_gain_hbm, first_gain),
+            (first_bias_hbm, first_bias), (router_hbm, router), (branch_hbm, branch),
+            (second_gain_hbm, second_gain), (second_bias_hbm, second_bias), (routes_hbm, routes),
+        )
+    ]
+    get_state = load(state_hbm, state)
+    get_dense = [load(dense_gate_hbm, dense_gate_w), load(dense_up_hbm, dense_up_w)]
+    get_wide = [load(gate_hbm, gate_w), load(up_hbm, up_w)]
+    get_down = [load(dense_down_hbm, dense_down_w), load(down_hbm, down_w)]
+
+    barrier = pltpu.get_barrier_semaphore()
+    for k in order:
+        pl.semaphore_signal(barrier, inc=1, device_id=(devices[k],), device_id_type=MESH)
+    pl.semaphore_signal(barrier, inc=1, device_id=(sibling,), device_id_type=MESH)
+    get_tokens.wait()
+    for copy in get_proj:
+        copy.wait()
+    get_mix.wait()
+    pl.semaphore_wait(barrier, chips)
+
+    sent = []
+
+    def spread(source, dest, send_sem, recv_sem):
+        for k in order:
+            copy = remote(source(k), dest.at[chip], send_sem.at[k], recv_sem.at[k], devices[k])
+            copy.start()
+            sent.append(copy)
+
+    def arrive(source, dest, send_sem, recv_sem):
+        for k in order:
+            remote(
+                source(k), dest.at[peers[k]], send_sem.at[k], recv_sem.at[k], devices[k]
+            ).wait_recv()
+
+    def swap(source, dest, i):
+        copy = remote(source, dest, pair_send.at[i], pair_recv.at[i], sibling)
+        copy.start()
+        sent.append(copy)
+
+    def swapped(source, dest, i):
+        remote(source, dest, pair_send.at[i], pair_recv.at[i], sibling).wait_recv()
+
+    own_tokens = lambda k: tok_blocks.at[chip]
+    spread(own_tokens, tok_blocks, a_send, a_recv)
+    for m in range(4):
+        swap(spots[m], spots[m], m)
+    swap(mix_spot, mix_spot, 4)
+
+    for copy in get_small:
+        copy.wait()
+    spread_rows = lambda rows: jnp.concatenate(
+        [jnp.broadcast_to(rows[h : h + 1], (nseq, depth)) for h in range(heads)], axis=0
+    )
+    bounds = spread_rows(bound[...])
+    branch_row = jnp.concatenate([branch[i : i + 1, :].astype(f32) for i in range(branch.shape[0])], axis=1)
+    small_w[...] = jnp.concatenate(
+        [router[...].astype(f32), branch_row, jnp.zeros((16 - EXPERTS - 1, width), f32)], axis=0
+    ).astype(bf16)
+
+    total = n * nseq
+    expert = lax.div(me, n // EXPERTS)
+    first, second = routes[0:1, :], routes[1:2, :]
+    ids = lax.broadcasted_iota(jnp.int32, (EXPERTS, total), 0)
+    gap = (first == ids).astype(f32) - (second == ids).astype(f32)
+    table = jnp.concatenate(
+        [gap, (first == expert).astype(f32), (second == expert).astype(f32),
+         jnp.zeros((16 - EXPERTS - 2, total), f32)], axis=0,
+    ).astype(bf16)
+    row = lax.broadcasted_iota(jnp.int32, (total, total), 0)
+    column = lax.broadcasted_iota(jnp.int32, (total, total), 1)
+    local = jnp.where(row < half, row, row - half)
+    parity = jnp.where(row < half, core, 1 - core)
+    which = (2 * (local // nseq) + parity) * nseq + local % nseq
+    turn = (which == column).astype(f32).astype(bf16)
+    picks = dot_turned(turn, table)
+
+    get_state.wait()
+    for p in range(heads // 2):
+        for q in range(nseq // 2):
+            for a in range(2):
+                for b in range(2):
+                    block = state[(2 * q + b) * heads + 2 * p + a]
+                    high = block.astype(bf16)
+                    low = (block - high.astype(f32)).astype(bf16)
+                    at = (p * (nseq // 2) + q, slice(a * depth, (a + 1) * depth), slice(b * depth, (b + 1) * depth))
+                    state_high[at] = high
+                    state_low[at] = low
+
+    arrive(own_tokens, tok_blocks, a_send, a_recv)
+    stack_rows(tok_blocks, tok_rows, chips, nseq)
+    for m in range(4):
+        swapped(spots[m], query_w.at[pl.ds(pl.multiple_of(m * 2 * own + (1 - core) * own, own), own)], m)
+    made = dot_turned(tok_rows[...], query_w[...])
+    for i in range(chips):
+        made_out[i] = made[i * nseq : (i + 1) * nseq].astype(bf16)
+    made_in[chip] = made_out[chip]
+    to_peer = lambda k: made_out.at[peers[k]]
+    spread(to_peer, made_in, b_send, b_recv)
+    arrive(to_peer, made_in, b_send, b_recv)
+
+    lane = lax.broadcasted_iota(jnp.int32, (nseq, depth), 1)
+    left = lane < depth // 2
+    parts = ([], [], [], [])
+    for h in range(heads):
+        one, two = made_in[2 * h].astype(f32), made_in[2 * h + 1].astype(f32)
+        for tile in range(2):
+            a = one[:, tile * depth : (tile + 1) * depth]
+            b = two[:, tile * depth : (tile + 1) * depth]
+            parts[2 * tile].append(jnp.where(left, a, pltpu.roll(b, depth // 2, 1)))
+            parts[2 * tile + 1].append(jnp.where(left, pltpu.roll(a, depth // 2, 1), b))
+    query, forget_in, value, outgate = [jnp.concatenate(part, axis=0) for part in parts]
+    forget = bounds + (1.0 - bounds) * jax.nn.sigmoid(forget_in)
+    keyed = (1.0 - bounds) * jax.nn.sigmoid(-forget_in)
+    aimed = query * forget
+    overlap = jnp.sum(query * keyed, axis=1, keepdims=True)
+    reads = []
+    seq = lax.broadcasted_iota(jnp.int32, (2 * nseq, depth), 0) % nseq
+    for p in range(heads // 2):
+        pair = aimed[p * 2 * nseq : (p + 1) * 2 * nseq]
+        zero = jnp.zeros((nseq, depth), f32)
+        wide = jnp.concatenate(
+            [jnp.concatenate([pair[:nseq], zero], axis=0), jnp.concatenate([zero, pair[nseq:]], axis=0)],
+            axis=1,
+        )
+        high = wide.astype(bf16).astype(f32)
+        lhs = jnp.concatenate([high, wide - high], axis=0).astype(bf16)
+        read = jnp.zeros((2 * nseq, depth), f32)
+        for q in range(nseq // 2):
+            at = p * (nseq // 2) + q
+            got = jnp.dot(lhs, state_high[at], preferred_element_type=f32)
+            got = got + jnp.dot(lhs, state_low[at], preferred_element_type=f32)
+            got = got[: 2 * nseq] + got[2 * nseq :]
+            for b in range(2):
+                read = jnp.where(seq == 2 * q + b, got[:, b * depth : (b + 1) * depth], read)
+        reads.append(read)
+    read = jnp.concatenate(reads, axis=0) + overlap * value
+    scaled = read * lax.rsqrt(jnp.mean(jnp.square(read), axis=-1, keepdims=True) + HEAD_EPS) * head_gain[...]
+    mixed = scaled * jax.nn.silu(outgate)
+    mix_blocks[chip] = jnp.concatenate(
+        [mixed[h * nseq : (h + 1) * nseq] for h in range(heads)], axis=1
+    ).astype(bf16)
+    own_mixed = lambda k: mix_blocks.at[chip]
+    spread(own_mixed, mix_blocks, c_send, c_recv)
+
+    tall = jnp.concatenate([forget, jnp.zeros((depth - heads * nseq, depth), f32)], axis=0).T
+    for h in range(heads):
+        for t in range(nseq):
+            i = h * nseq + t
+            here = value[i : i + 1]
+            fresh_ref[t * heads + h] = here + tall[:, i : i + 1] * (state[t * heads + h] - here)
+
+    arrive(own_mixed, mix_blocks, c_send, c_recv)
+    stack_rows(mix_blocks, mix_rows, chips, nseq)
+    swapped(mix_spot, mix_w.at[pl.ds(pl.multiple_of((1 - core) * mix_own, mix_own), mix_own)], 4)
+    feats[chip] = dot_turned(mix_rows[...], mix_w[...]).astype(bf16)
+    own_feats = lambda k: feats.at[chip]
+    spread(own_feats, feats, d_send, d_recv)
+    arrive(own_feats, feats, d_send, d_recv)
+
+    for g in range(half // 16):
+        rows = slice(g * 16, (g + 1) * 16)
+        mixture = ALPHA * tok_rows[rows, :].astype(f32) + jnp.concatenate(
+            [feats[c, rows, :].astype(f32) for c in range(chips)], axis=1
+        )
+        normed[rows, :] = layer_norm(mixture, first_gain[...], first_bias[...]).astype(bf16)
+        swap(normed.at[rows], normed.at[half + g * 16 : half + (g + 1) * 16], 5 + g)
+    for g in range(half // 16):
+        rows = slice(g * 16, (g + 1) * 16)
+        swapped(normed.at[rows], normed.at[half + g * 16 : half + (g + 1) * 16], 5 + g)
+    swaps = 5 + half // 16
+
+    x = normed[...]
+    small = dot_turned(x, small_w[...])
+    share = jax.nn.sigmoid(jnp.sum(small[:, :EXPERTS] * picks[:, :EXPERTS], axis=1, keepdims=True))
+    branch_gate = jax.nn.sigmoid(small[:, EXPERTS : EXPERTS + 1])
+    on_first = picks[:, EXPERTS : EXPERTS + 1] > 0
+    on_second = picks[:, EXPERTS + 1 : EXPERTS + 2] > 0
+    weight = jnp.where(on_first, share, jnp.where(on_second, 1.0 - share, 0.0))
+    dot = functools.partial(jnp.dot, preferred_element_type=f32)
+    for copy in get_dense:
+        copy.wait()
+    gate_part = dot_turned(x, dense_gate_w[...])
+    up_part = dot_turned(x, dense_up_w[...])
+    dense_hidden[...] = (jax.nn.silu(gate_part) * up_part).astype(bf16)
+    for copy in get_wide:
+        copy.wait()
+    tile = column_tile(hidden.shape[1])
+    for i in range(hidden.shape[1] // tile):
+        at = slice(i * tile, (i + 1) * tile)
+        gate_part = dot(normed[...], gate_w[:, at])
+        up_part = dot(normed[...], up_w[:, at])
+        hidden[:, at] = (jax.nn.silu(gate_part) * up_part).astype(bf16)
+    for copy in get_down:
+        copy.wait()
+
+    step = width // chunks
+    for j in range(chunks):
+        tile = min(step, 256)
+        for i in range(step // tile):
+            at = slice(j * step + i * tile, j * step + (i + 1) * tile)
+            routed = dot(hidden[...], down_w[:, at])
+            dense = dot(dense_hidden[...], dense_down_w[:, at])
+            made = branch_gate * dense + jnp.where(weight > 0, weight * routed, 0.0)
+            own_part[:, at] = made[:half]
+            pair_out[j, :, i * tile : (i + 1) * tile] = made[half:].astype(bf16)
+        swap(pair_out.at[j], pair_in.at[j], swaps + j)
+    for j in range(chunks):
+        swapped(pair_out.at[j], pair_in.at[j], swaps + j)
+        at = slice(j * step, (j + 1) * step)
+        both = own_part[:, at] + pair_in[j].astype(f32)
+        for i in range(chips):
+            outgoing[j, i] = both[i * nseq : (i + 1) * nseq].astype(bf16)
+        spread(lambda k: outgoing.at[j, peers[k]], landed.at[j], f_send.at[j], f_recv.at[j])
+        landed[j, chip] = outgoing[j, chip]
+
+    base = pl.multiple_of(lax.div(chip * nseq, 16) * 16, 16)
+    around = normed[pl.ds(base, 16), :].astype(f32)
+    place = lax.broadcasted_iota(jnp.int32, (16, width), 0) // nseq
+    kept = jnp.where(place == lax.rem(chip, 16 // nseq), around, 0.0)
+    residual = sum(kept[i * nseq : (i + 1) * nseq] for i in range(16 // nseq))
+    sums = []
+    for j in range(chunks):
+        arrive(lambda k: outgoing.at[j, peers[k]], landed.at[j], f_send.at[j], f_recv.at[j])
+        sums.append(sum(landed[j, i].astype(f32) for i in range(chips)))
+    mixture = ALPHA * residual + jnp.concatenate(sums, axis=1)
+    out_ref[...] = layer_norm(mixture, second_gain[...], second_bias[...]).astype(bf16)
+    for copy in sent:
+        copy.wait_send()
+
+
+def fits(n, tokens, query_weight, mixout_weight, bound, depth):
+    chips = n // 2
+    nseq = tokens.shape[0]
+    return (
+        n % 2 == 0
+        and chips & (chips - 1) == 0
+        and n % EXPERTS == 0
+        and nseq % 2 == 0
+        and 16 % nseq == 0
+        and (chips * nseq) % 16 == 0
+        and 2 * mixout_weight.shape[1] == 128
+        and 2 * query_weight.shape[1] == depth // 2
+        and depth == 128
+        and bound.shape[0] // depth * nseq <= depth
+        and n * nseq == 128
+        and tokens.shape[1] % 512 == 0
+    )
+
+
+def whole_layer(
+    tokens, recurrent_state, query_weight, forget_weight, input_weight, outgate_weight,
+    lower_bound, head_gain, mixout_weight, first_gain, first_bias, router_weight, branch_vector,
+    dense_gate_weight, dense_up_weight, dense_down_weight, expert_gate_weight, expert_up_weight,
+    expert_down_weight, second_gain, second_bias, routes,
+):
+    bf16, f32 = jnp.bfloat16, jnp.float32
+    n = lax.axis_size("ep")
+    chips = n // 2
+    nseq, width = tokens.shape
+    _, heads, depth, _ = recurrent_state.shape
+    chunks = CHUNKS
+    half = chips * nseq
+    own, mix_own = query_weight.shape[1], mixout_weight.shape[1]
+    operands = (
+        tokens, recurrent_state.reshape(nseq * heads, depth, depth),
+        query_weight.T, forget_weight.T, input_weight.T, outgate_weight.T,
+        lower_bound.reshape(heads, depth), head_gain[None], mixout_weight.T,
+        first_gain[None], first_bias[None], router_weight.T, branch_vector.reshape(-1, 128),
+        dense_gate_weight.T, dense_up_weight.T, dense_down_weight,
+        expert_gate_weight, expert_up_weight, expert_down_weight,
+        second_gain[None], second_bias[None], routes.T,
+    )
+    (
+        _, state, query, *_, bound, head, mix, gain1, bias1, router, branch,
+        dgate, dup, ddown, gate, up, down, gain2, bias2, route,
+    ) = operands
+    vmem = lambda a: pltpu.VMEM(a.shape, a.dtype)
+    sems = lambda *shape: pltpu.SemaphoreType.DMA(shape)
+    pairs = 5 + half // 16 + chunks
+    output, fresh = pl.pallas_call(
+        functools.partial(layer_kernel, n, chunks),
+        out_shape=(
+            jax.ShapeDtypeStruct((nseq, width), bf16),
+            jax.ShapeDtypeStruct(state.shape, f32),
+        ),
+        in_specs=[pl.BlockSpec(memory_space=pltpu.HBM)] * len(operands),
+        out_specs=(pl.BlockSpec(memory_space=pltpu.VMEM), pl.BlockSpec(memory_space=pltpu.VMEM)),
+        scratch_shapes=[
+            vmem(state), pltpu.VMEM((8 * own, width), bf16),
+            pltpu.VMEM((2 * mix_own, mix.shape[1]), bf16),
+            *[vmem(a) for a in (gate, up, down, dgate, dup, ddown)],
+            *[vmem(a) for a in (bound, head, gain1, bias1, router, branch, gain2, bias2, route)],
+            pltpu.VMEM((chips, nseq, width), bf16), pltpu.VMEM((half, width), bf16),
+            pltpu.VMEM((chips, nseq, 8 * own), bf16), pltpu.VMEM((chips, nseq, 8 * own), bf16),
+            pltpu.VMEM((chips, nseq, mix.shape[1]), bf16), pltpu.VMEM((half, mix.shape[1]), bf16),
+            pltpu.VMEM((chips, half, 2 * mix_own), bf16), pltpu.VMEM((2 * half, width), bf16),
+            pltpu.VMEM((heads * nseq // 4, 2 * depth, 2 * depth), bf16),
+            pltpu.VMEM((heads * nseq // 4, 2 * depth, 2 * depth), bf16),
+            pltpu.VMEM((16, width), bf16),
+            pltpu.VMEM((2 * half, gate.shape[1]), bf16), pltpu.VMEM((2 * half, dgate.shape[0]), bf16),
+            pltpu.VMEM((half, width), f32),
+            pltpu.VMEM((chunks, half, width // chunks), bf16),
+            pltpu.VMEM((chunks, half, width // chunks), bf16),
+            pltpu.VMEM((chunks, chips, nseq, width // chunks), bf16),
+            pltpu.VMEM((chunks, chips, nseq, width // chunks), bf16),
+            sems(len(operands)),
+            *[sems(chips)] * 8, sems(chunks, chips), sems(chunks, chips), sems(pairs), sems(pairs),
+        ],
+        compiler_params=pltpu.CompilerParams(
+            collective_id=3, has_side_effects=True, vmem_limit_bytes=44 * 2**20
+        ),
+    )(*operands)
+    return output, fresh.reshape(recurrent_state.shape)
+
+
 def per_device(
     tokens,
     recurrent_state,
@@ -361,6 +751,16 @@
 ):
     f32 = jnp.float32
     devices = lax.axis_size("ep")
+    if fits(
+        devices, tokens, query_weight, mixout_weight, lower_bound, recurrent_state.shape[-1]
+    ):
+        return whole_layer(
+            tokens, recurrent_state, query_weight, forget_weight, input_weight, outgate_weight,
+            lower_bound, head_gain, mixout_weight, first_gain, first_bias, router_weight,
+            branch_vector, dense_gate_weight, dense_up_weight, dense_down_weight,
+            expert_gate_weight, expert_up_weight, expert_down_weight, second_gain, second_bias,
+            routes,
+        )
     nseq, width = tokens.shape
     own_cols = query_weight.shape[1]
     stacked = jnp.concatenate(

time: 82 us -> 71.1 us (0.87)
  the two profiles are of different devices: /device:TPU:29 before, /device:TPU:0 now
where the time goes in v1:
time: 71.1 us; the launch traced here: 70.3 us
  Pallas kernels  51.3 us (72%)
  local copies, waits for them, and re-layouts  18.3 us (26%)
    pallas_call x1, Pallas kernels, whole_layer(): pl.pallas_call(functools.partial(layer_kernel, n, chunks), out_shape=(jax...  51.3 us
    unnamed x40, local copies, waits for them, and re-layouts  18.3 us

profile of v1, /device:TPU:0, one launch (start us, length us, event | category | flops | bytes accessed | tf_op | source)
XLA Modules:
  0.0 70.3 jit_solution(2684235402687991618)
XLA Ops:
  0.6 0.0 copy-start
  0.6 1.6 %copy-done = f32[4,8,128,128]{3,2,1,0:T(8,128)S(1)} copy-done((f32[4,8,128,128]{3,2,1,0:T(8,128)S(1)}, f32[4,8,128,128]{3,2,1,0:T(8,128)}, u32[]{:S(2)}) %copy-start) | copy-done | bytes 2097176
  2.2 0.0 copy-start.1
  2.2 1.1 %copy-done.1 = bf16[2048,176]{0,1:T(8,128)(2,1)S(1)} copy-done((bf16[2048,176]{0,1:T(8,128)(2,1)S(1)}, bf16[2048,176]{0,1:T(8,128)(2,1)}, u32[]{:S(2)}) %copy-start.1) | copy-done | bytes 720920
  3.3 0.0 copy-start.2
  3.3 1.1 %copy-done.2 = bf16[2048,176]{0,1:T(8,128)(2,1)S(1)} copy-done((bf16[2048,176]{0,1:T(8,128)(2,1)S(1)}, bf16[2048,176]{0,1:T(8,128)(2,1)}, u32[]{:S(2)}) %copy-start.2) | copy-done | bytes 720920
  4.5 0.0 copy-start.3
  4.5 1.1 %copy-done.3 = bf16[176,2048]{1,0:T(8,128)(2,1)S(1)} copy-done((bf16[176,2048]{1,0:T(8,128)(2,1)S(1)}, bf16[176,2048]{1,0:T(8,128)(2,1)}, u32[]{:S(2)}) %copy-start.3) | copy-done | bytes 720920
  5.6 0.0 copy-start.4
  5.6 0.9 %copy-done.4 = bf16[2048,32]{0,1:T(8,128)(2,1)S(1)} copy-done((bf16[2048,32]{0,1:T(8,128)(2,1)S(1)}, bf16[2048,32]{0,1:T(8,128)(2,1)}, u32[]{:S(2)}) %copy-start.4) | copy-done | bytes 131096
  6.5 0.0 copy-start.5
  6.5 0.9 %copy-done.5 = bf16[2048,32]{0,1:T(8,128)(2,1)S(1)} copy-done((bf16[2048,32]{0,1:T(8,128)(2,1)S(1)}, bf16[2048,32]{0,1:T(8,128)(2,1)}, u32[]{:S(2)}) %copy-start.5) | copy-done | bytes 131096
  7.4 0.0 copy-start.6
  7.4 0.9 %copy-done.6 = bf16[2048,32]{0,1:T(8,128)(2,1)S(1)} copy-done((bf16[2048,32]{0,1:T(8,128)(2,1)S(1)}, bf16[2048,32]{0,1:T(8,128)(2,1)}, u32[]{:S(2)}) %copy-start.6) | copy-done | bytes 131096
  8.3 0.0 copy-start.7
  8.3 0.9 %copy-done.7 = bf16[2048,32]{0,1:T(8,128)(2,1)S(1)} copy-done((bf16[2048,32]{0,1:T(8,128)(2,1)S(1)}, bf16[2048,32]{0,1:T(8,128)(2,1)}, u32[]{:S(2)}) %copy-start.7) | copy-done | bytes 131096
  9.2 0.0 copy-start.8
  9.2 0.9 %copy-done.8 = bf16[1024,64]{0,1:T(8,128)(2,1)S(1)} copy-done((bf16[1024,64]{0,1:T(8,128)(2,1)S(1)}, bf16[1024,64]{0,1:T(8,128)(2,1)}, u32[]{:S(2)}) %copy-start.8) | copy-done | bytes 131096
  10.1 0.0 copy-start.9
  10.1 0.8 %copy-done.9 = bf16[2048,8]{0,1:T(8,128)(2,1)S(1)} copy-done((bf16[2048,8]{0,1:T(8,128)(2,1)S(1)}, bf16[2048,8]{0,1:T(8,128)(2,1)}, u32[]{:S(2)}) %copy-start.9) | copy-done | bytes 32792
  10.8 0.0 copy-start.10
  10.8 0.7 %copy-done.10 = bf16[4,2048]{1,0:T(4,128)(2,1)S(1)} copy-done((bf16[4,2048]{1,0:T(4,128)(2,1)S(1)}, bf16[4,2048]{1,0:T(4,128)(2,1)}, u32[]{:S(2)}) %copy-start.10) | copy-done | bytes 16408
  11.6 0.0 copy-start.11
  11.6 0.7 copy-done.11
  12.3 0.0 copy-start.12
  12.3 0.7 copy-done.12
  13.0 0.0 copy-start.13
  13.0 0.7 copy-done.13
  13.7 0.0 copy-start.14
  13.7 0.7 copy-done.14
  14.4 0.0 copy-start.15
  14.4 0.7 copy-done.15
  15.0 0.0 copy-start.16
  15.0 0.7 copy-done.16
  15.7 0.0 copy-start.17
  15.7 0.7 copy-done.17
  16.4 0.0 copy-start.18
  16.4 0.7 copy-done.18
  17.1 51.3 %shard_map.221 = (bf16[4,2048]{1,0:T(4,128)(2,1)S(1)}, f32[32,128,128]{2,1,0:T(8,128)S(1)}) custom-call(bf16[4,2048]{1,0:T(4,128)(2,1)S(1)} %copy-done.10, f32[32,128,128]{2,1,0:T(8,128)S(1)} %bitcast.18, bf16[32,2048]{1,0:T(8,128)(2,1)S(1)} %bitcast.22, bf16[32,2048]{1,0:T(8,128)(2,1)S(1)} %bitcast.23, bf16[32,2048]{1,0:T(8,128)(2,1)S(1)} %bitcast.24, ...), custom_call_target="tpu_custom_call" | custom-call | tf_op jit(solution)/shard_map/pallas_call | solution.py:692
  68.4 0.6 copy.26
  69.0 1.3 %copy.27 = f32[4,8,128,128]{3,2,1,0:T(8,128)} copy(f32[4,8,128,128]{3,2,1,0:T(8,128)S(1)} %bitcast.19) | data formatting | bytes 4194304
Async XLA Ops:
  0.6 1.6 %copy-start = (f32[4,8,128,128]{3,2,1,0:T(8,128)S(1)}, f32[4,8,128,128]{3,2,1,0:T(8,128)}, u32[]{:S(2)}) copy-start(f32[4,8,128,128]{3,2,1,0:T(8,128)} %param.23) | copy-start | bytes 6291460
  2.2 1.1 %copy-start.1 = (bf16[2048,176]{0,1:T(8,128)(2,1)S(1)}, bf16[2048,176]{0,1:T(8,128)(2,1)}, u32[]{:S(2)}) copy-start(bf16[2048,176]{0,1:T(8,128)(2,1)} %param.35) | copy-start | bytes 2162692
  3.3 1.1 %copy-start.2 = (bf16[2048,176]{0,1:T(8,128)(2,1)S(1)}, bf16[2048,176]{0,1:T(8,128)(2,1)}, u32[]{:S(2)}) copy-start(bf16[2048,176]{0,1:T(8,128)(2,1)} %param.36) | copy-start | bytes 2162692
  4.5 1.1 %copy-start.3 = (bf16[176,2048]{1,0:T(8,128)(2,1)S(1)}, bf16[176,2048]{1,0:T(8,128)(2,1)}, u32[]{:S(2)}) copy-start(bf16[176,2048]{1,0:T(8,128)(2,1)} %dense_down_hbm.1) | copy-start | bytes 2162692
  5.6 0.9 %copy-start.4 = (bf16[2048,32]{0,1:T(8,128)(2,1)S(1)}, bf16[2048,32]{0,1:T(8,128)(2,1)}, u32[]{:S(2)}) copy-start(bf16[2048,32]{0,1:T(8,128)(2,1)} %param.24) | copy-start | bytes 393220
  6.5 0.9 %copy-start.5 = (bf16[2048,32]{0,1:T(8,128)(2,1)S(1)}, bf16[2048,32]{0,1:T(8,128)(2,1)}, u32[]{:S(2)}) copy-start(bf16[2048,32]{0,1:T(8,128)(2,1)} %param.25) | copy-start | bytes 393220
  7.4 0.9 %copy-start.6 = (bf16[2048,32]{0,1:T(8,128)(2,1)S(1)}, bf16[2048,32]{0,1:T(8,128)(2,1)}, u32[]{:S(2)}) copy-start(bf16[2048,32]{0,1:T(8,128)(2,1)} %param.26) | copy-start | bytes 393220
  8.3 0.9 %copy-start.7 = (bf16[2048,32]{0,1:T(8,128)(2,1)S(1)}, bf16[2048,32]{0,1:T(8,128)(2,1)}, u32[]{:S(2)}) copy-start(bf16[2048,32]{0,1:T(8,128)(2,1)} %param.27) | copy-start | bytes 393220
  9.2 0.9 %copy-start.8 = (bf16[1024,64]{0,1:T(8,128)(2,1)S(1)}, bf16[1024,64]{0,1:T(8,128)(2,1)}, u32[]{:S(2)}) copy-start(bf16[1024,64]{0,1:T(8,128)(2,1)} %param.30) | copy-start | bytes 393220
  10.1 0.8 %copy-start.9 = (bf16[2048,8]{0,1:T(8,128)(2,1)S(1)}, bf16[2048,8]{0,1:T(8,128)(2,1)}, u32[]{:S(2)}) copy-start(bf16[2048,8]{0,1:T(8,128)(2,1)} %param.33) | copy-start | bytes 98308
  10.8 0.7 %copy-start.10 = (bf16[4,2048]{1,0:T(4,128)(2,1)S(1)}, bf16[4,2048]{1,0:T(4,128)(2,1)}, u32[]{:S(2)}) copy-start(bf16[4,2048]{1,0:T(4,128)(2,1)} %tokens_hbm.1) | copy-start | bytes 49156
  11.6 0.7 copy-start.11
  12.3 0.7 copy-start.12
  13.0 0.7 copy-start.13
  13.7 0.7 copy-start.14
  14.4 0.7 copy-start.15
  15.0 0.7 copy-start.16
  15.7 0.7 copy-start.17
  16.4 0.7 copy-start.18

commit v2 on v1

--- a/solution.py
+++ b/solution.py
@@ -9,6 +9,7 @@
 
 EXPERTS = 8
 CHUNKS = 4
+PLANE = 4
 MESH = pl.DeviceIdType.MESH
 
 
@@ -368,14 +369,14 @@
     tokens_hbm, state_hbm, query_hbm, forget_hbm, value_hbm, outgate_hbm, bound_hbm, head_gain_hbm,
     mixout_hbm, first_gain_hbm, first_bias_hbm, router_hbm, branch_hbm,
     dense_gate_hbm, dense_up_hbm, dense_down_hbm, gate_hbm, up_hbm, down_hbm,
-    second_gain_hbm, second_bias_hbm, routes_hbm,
+    routes_hbm,
     out_ref, fresh_ref,
-    state, query_w, mix_w, gate_w, up_w, down_w, dense_gate_w, dense_up_w, dense_down_w,
-    bound, head_gain, first_gain, first_bias, router, branch, second_gain, second_bias, routes,
-    tok_blocks, tok_rows, made_out, made_in, mix_blocks, mix_rows, feats, normed,
+    state, query_w, mix_w, wide_w, down_w, dense_w, dense_down_w,
+    bound, head_gain, first_gain, first_bias, router, branch, routes,
+    tok_blocks, tok_rows, made_out, made_in, mix_blocks, mix_rows, feats, stretched, normed,
     state_high, state_low, small_w, hidden, dense_hidden, own_part, pair_out, pair_in,
     outgoing, landed,
-    load_sem, a_send, a_recv, b_send, b_recv, c_send, c_recv, d_send, d_recv, f_send, f_recv,
+    ready, load_sem, a_send, a_recv, b_send, b_recv, c_send, c_recv, d_send, d_recv, f_send, f_recv,
     pair_send, pair_recv,
 ):
     bf16, f32 = jnp.bfloat16, jnp.float32
@@ -393,70 +394,108 @@
     mix_own = mixout_hbm.shape[0]
     at_core = lambda base, size: pl.ds(pl.multiple_of(base + core * size, size), size)
 
-    loads = []
-
-    def load(there, here):
-        copy = pltpu.make_async_copy(there, here, load_sem.at[len(loads)])
+    def load(there, here, i):
+        copy = pltpu.make_async_copy(there, here, load_sem.at[i])
         copy.start()
-        loads.append(copy)
         return copy
 
-    get_tokens = load(tokens_hbm, tok_blocks.at[chip])
+    def drain(ref, sem):
+        pltpu.make_async_copy(ref, ref, sem).wait()
+
+    get_tokens = load(tokens_hbm, tok_blocks.at[chip], 0)
     pieces = (query_hbm, forget_hbm, value_hbm, outgate_hbm)
     spots = [query_w.at[at_core(m * 2 * own, own)] for m in range(4)]
-    get_proj = [load(piece, spot) for piece, spot in zip(pieces, spots)]
+    for piece, spot in zip(pieces, spots):
+        load(piece, spot, 1)
     mix_spot = mix_w.at[at_core(0, mix_own)]
-    get_mix = load(mixout_hbm, mix_spot)
+    get_mix = load(mixout_hbm, mix_spot, 2)
+    get_state = load(state_hbm, state, 3)
     get_small = [
-        load(there, here)
-        for there, here in (
+        load(there, here, 4 + i)
+        for i, (there, here) in enumerate((
             (bound_hbm, bound), (head_gain_hbm, head_gain), (first_gain_hbm, first_gain),
             (first_bias_hbm, first_bias), (router_hbm, router), (branch_hbm, branch),
-            (second_gain_hbm, second_gain), (second_bias_hbm, second_bias), (routes_hbm, routes),
-        )
+            (routes_hbm, routes),
+        ))
     ]
-    get_state = load(state_hbm, state)
-    get_dense = [load(dense_gate_hbm, dense_gate_w), load(dense_up_hbm, dense_up_w)]
-    get_wide = [load(gate_hbm, gate_w), load(up_hbm, up_w)]
-    get_down = [load(dense_down_hbm, dense_down_w), load(down_hbm, down_w)]
+    load(dense_gate_hbm, dense_w.at[0], 11)
+    load(dense_up_hbm, dense_w.at[1], 11)
+    load(gate_hbm, wide_w.at[0], 12)
+    load(up_hbm, wide_w.at[1], 12)
+    get_down = [load(dense_down_hbm, dense_down_w, 13), load(down_hbm, down_w, 14)]
 
     barrier = pltpu.get_barrier_semaphore()
-    for k in order:
-        pl.semaphore_signal(barrier, inc=1, device_id=(devices[k],), device_id_type=MESH)
+    above = [peer > chip for peer in peers]
+    partners = [k for k in range(1, chips) if k < PLANE or k % PLANE == 0]
     pl.semaphore_signal(barrier, inc=1, device_id=(sibling,), device_id_type=MESH)
-    get_tokens.wait()
-    for copy in get_proj:
-        copy.wait()
-    get_mix.wait()
-    pl.semaphore_wait(barrier, chips)
+    for k in partners:
+
+        @pl.when(above[k])
+        def _(k=k):
+            pl.semaphore_signal(barrier, inc=1, device_id=(devices[k],), device_id_type=MESH)
+
+    pl.semaphore_wait(barrier, lax.div(chip, PLANE) + lax.rem(chip, PLANE) + 1)
+    for k in partners:
+
+        @pl.when(jnp.logical_not(above[k]))
+        def _(k=k):
+            pl.semaphore_signal(ready.at[partners.index(k)], inc=1, device_id=(devices[k],), device_id_type=MESH)
 
     sent = []
 
     def spread(source, dest, send_sem, recv_sem):
         for k in order:
-            copy = remote(source(k), dest.at[chip], send_sem.at[k], recv_sem.at[k], devices[k])
-            copy.start()
-            sent.append(copy)
-
-    def arrive(source, dest, send_sem, recv_sem):
-        for k in order:
-            remote(
-                source(k), dest.at[peers[k]], send_sem.at[k], recv_sem.at[k], devices[k]
-            ).wait_recv()
+            remote(source(k), dest.at[chip], send_sem, recv_sem, devices[k]).start()
+        sent.append((dest.at[: chips - 1], send_sem))
+
+    def arrive(dest, recv_sem):
+        drain(dest.at[: chips - 1], recv_sem)
+
+    lines = range(PLANE, chips, PLANE)
+    others = chips // PLANE * (PLANE - 1)
+
+    def step_copy(blocks, send_sem, recv_sem, line, k, device=None):
+        block = blocks.at[peers[line]]
+        device = devices[k] if device is None else device
+        return remote(block, block, send_sem, recv_sem.at[k // PLANE], device)
+
+    def landing(blocks, send_sem, recv_sem, line):
+        remote(
+            blocks.at[chip], blocks.at[peers[line]], send_sem, recv_sem.at[line // PLANE], devices[line]
+        ).wait_recv()
+
+    def onward(blocks, send_sem, recv_sem):
+        for line in lines:
+            landing(blocks, send_sem, recv_sem, line)
+            for k in range(1, PLANE):
+                step_copy(blocks, send_sem, recv_sem, line, k).start()
 
     def swap(source, dest, i):
-        copy = remote(source, dest, pair_send.at[i], pair_recv.at[i], sibling)
-        copy.start()
-        sent.append(copy)
-
-    def swapped(source, dest, i):
-        remote(source, dest, pair_send.at[i], pair_recv.at[i], sibling).wait_recv()
-
-    own_tokens = lambda k: tok_blocks.at[chip]
-    spread(own_tokens, tok_blocks, a_send, a_recv)
+        remote(source, dest, pair_send.at[i], pair_recv.at[i], sibling).start()
+
+    get_tokens.wait()
+    for k in reversed(partners):
+
+        @pl.when(jnp.logical_not(above[k]))
+        def _(k=k):
+            step_copy(tok_blocks, a_send, a_recv, 0, k).start()
+
+    for k in partners:
+
+        @pl.when(above[k])
+        def _(k=k):
+            pl.semaphore_wait(ready.at[partners.index(k)], 1)
+            step_copy(tok_blocks, a_send, a_recv, 0, k).start()
+    drain(query_w.at[: 4 * own], load_sem.at[1])
     for m in range(4):
-        swap(spots[m], spots[m], m)
-    swap(mix_spot, mix_spot, 4)
+        swap(spots[m], spots[m], 0)
+    sent.append((query_w.at[: 4 * own], pair_send.at[0]))
+    get_mix.wait()
+    swap(mix_spot, mix_spot, 1)
+    sent.append((mix_spot, pair_send.at[1]))
+
+    onward(tok_blocks, a_send, a_recv)
+    sent.append((tok_blocks.at[: chips - 1], a_send))
 
     for copy in get_small:
         copy.wait()
@@ -498,17 +537,17 @@
                     state_high[at] = high
                     state_low[at] = low
 
-    arrive(own_tokens, tok_blocks, a_send, a_recv)
+    drain(tok_blocks.at[:others], a_recv.at[0])
     stack_rows(tok_blocks, tok_rows, chips, nseq)
-    for m in range(4):
-        swapped(spots[m], query_w.at[pl.ds(pl.multiple_of(m * 2 * own + (1 - core) * own, own), own)], m)
+    drain(query_w.at[: 4 * own], pair_recv.at[0])
     made = dot_turned(tok_rows[...], query_w[...])
     for i in range(chips):
         made_out[i] = made[i * nseq : (i + 1) * nseq].astype(bf16)
     made_in[chip] = made_out[chip]
     to_peer = lambda k: made_out.at[peers[k]]
     spread(to_peer, made_in, b_send, b_recv)
-    arrive(to_peer, made_in, b_send, b_recv)
+    stretched[...] = ALPHA * tok_rows[...].astype(f32)
+    arrive(made_in, b_recv)
 
     lane = lax.broadcasted_iota(jnp.int32, (nseq, depth), 1)
     left = lane < depth // 2
@@ -561,25 +600,54 @@
             here = value[i : i + 1]
             fresh_ref[t * heads + h] = here + tall[:, i : i + 1] * (state[t * heads + h] - here)
 
-    arrive(own_mixed, mix_blocks, c_send, c_recv)
+    arrive(mix_blocks, c_recv)
     stack_rows(mix_blocks, mix_rows, chips, nseq)
-    swapped(mix_spot, mix_w.at[pl.ds(pl.multiple_of((1 - core) * mix_own, mix_own), mix_own)], 4)
+    drain(mix_spot, pair_recv.at[1])
     feats[chip] = dot_turned(mix_rows[...], mix_w[...]).astype(bf16)
-    own_feats = lambda k: feats.at[chip]
-    spread(own_feats, feats, d_send, d_recv)
-    arrive(own_feats, feats, d_send, d_recv)
-
-    for g in range(half // 16):
-        rows = slice(g * 16, (g + 1) * 16)
-        mixture = ALPHA * tok_rows[rows, :].astype(f32) + jnp.concatenate(
-            [feats[c, rows, :].astype(f32) for c in range(chips)], axis=1
+    @pl.when(core == 1)
+    def _():
+        for k in partners:
+            step_copy(feats, d_send, d_recv, 0, k).start()
+        onward(feats, d_send, d_recv)
+
+    @pl.when(core == 0)
+    def _():
+        for k in order:
+            step_copy(feats, d_send, d_recv, 0, k if k % PLANE == 0 else k % PLANE, devices[k]).start()
+        for line in lines:
+            landing(feats, d_send, d_recv, line)
+
+    sent.append((feats.at[: chips - 1], d_send))
+
+    lanes = 2 * mix_own
+
+    def take(c):
+        at = pl.ds(pl.multiple_of(c * lanes, lanes), lanes)
+        value = stretched[:, at] + feats[c].astype(f32)
+        stretched[:, at] = value
+        return value
+
+    total = take(chip)
+    for line in lines:
+        total = total + take(peers[line])
+    drain(feats.at[:others], d_recv.at[0])
+    for k in range(1, chips):
+        if k % PLANE:
+            total = total + take(peers[k])
+    center = jnp.sum(total, axis=1, keepdims=True) * (1.0 / width)
+    groups = [slice(g * 16, (g + 1) * 16) for g in range(half // 16)]
+    spreads = [
+        lax.rsqrt(
+            jnp.mean(jnp.square(stretched[rows, :] - center[rows]), axis=1, keepdims=True) + NORM_EPS
         )
-        normed[rows, :] = layer_norm(mixture, first_gain[...], first_bias[...]).astype(bf16)
-        swap(normed.at[rows], normed.at[half + g * 16 : half + (g + 1) * 16], 5 + g)
-    for g in range(half // 16):
-        rows = slice(g * 16, (g + 1) * 16)
-        swapped(normed.at[rows], normed.at[half + g * 16 : half + (g + 1) * 16], 5 + g)
-    swaps = 5 + half // 16
+        for rows in groups
+    ]
+    for g, rows in enumerate(groups):
+        row = (stretched[rows, :] - center[rows]) * spreads[g] * first_gain[...] + first_bias[...]
+        normed[rows, :] = row.astype(bf16)
+        swap(normed.at[rows], normed.at[half + g * 16 : half + (g + 1) * 16], 2)
+    sent.append((normed.at[:half], pair_send.at[2]))
+    drain(normed.at[half:], pair_recv.at[2])
 
     x = normed[...]
     small = dot_turned(x, small_w[...])
@@ -589,18 +657,16 @@
     on_second = picks[:, EXPERTS + 1 : EXPERTS + 2] > 0
     weight = jnp.where(on_first, share, jnp.where(on_second, 1.0 - share, 0.0))
     dot = functools.partial(jnp.dot, preferred_element_type=f32)
-    for copy in get_dense:
-        copy.wait()
-    gate_part = dot_turned(x, dense_gate_w[...])
-    up_part = dot_turned(x, dense_up_w[...])
+    drain(dense_w, load_sem.at[11])
+    gate_part = dot_turned(x, dense_w[0])
+    up_part = dot_turned(x, dense_w[1])
     dense_hidden[...] = (jax.nn.silu(gate_part) * up_part).astype(bf16)
-    for copy in get_wide:
-        copy.wait()
+    drain(wide_w, load_sem.at[12])
     tile = column_tile(hidden.shape[1])
     for i in range(hidden.shape[1] // tile):
         at = slice(i * tile, (i + 1) * tile)
-        gate_part = dot(normed[...], gate_w[:, at])
-        up_part = dot(normed[...], up_w[:, at])
+        gate_part = dot(normed[...], wide_w[0, :, at])
+        up_part = dot(normed[...], wide_w[1, :, at])
         hidden[:, at] = (jax.nn.silu(gate_part) * up_part).astype(bf16)
     for copy in get_down:
         copy.wait()
@@ -615,9 +681,10 @@
             made = branch_gate * dense + jnp.where(weight > 0, weight * routed, 0.0)
             own_part[:, at] = made[:half]
             pair_out[j, :, i * tile : (i + 1) * tile] = made[half:].astype(bf16)
-        swap(pair_out.at[j], pair_in.at[j], swaps + j)
+        swap(pair_out.at[j], pair_in.at[j], 3 + j)
+        sent.append((pair_out.at[j], pair_send.at[3 + j]))
     for j in range(chunks):
-        swapped(pair_out.at[j], pair_in.at[j], swaps + j)
+        drain(pair_in.at[j], pair_recv.at[3 + j])
         at = slice(j * step, (j + 1) * step)
         both = own_part[:, at] + pair_in[j].astype(f32)
         for i in range(chips):
@@ -632,12 +699,22 @@
     residual = sum(kept[i * nseq : (i + 1) * nseq] for i in range(16 // nseq))
     sums = []
     for j in range(chunks):
-        arrive(lambda k: outgoing.at[j, peers[k]], landed.at[j], f_send.at[j], f_recv.at[j])
+        arrive(landed.at[j], f_recv.at[j])
         sums.append(sum(landed[j, i].astype(f32) for i in range(chips)))
     mixture = ALPHA * residual + jnp.concatenate(sums, axis=1)
-    out_ref[...] = layer_norm(mixture, second_gain[...], second_bias[...]).astype(bf16)
-    for copy in sent:
-        copy.wait_send()
+    out_ref[...] = mixture
+    for ref, sem in sent:
+        drain(ref, sem)
+
+
+def finish_kernel(mixture, fresh, gain, bias, out_hbm, state_hbm, rows, sem):
+    keep = pltpu.make_async_copy(fresh, state_hbm, sem.at[0])
+    keep.start()
+    rows[...] = layer_norm(mixture[...], gain[...], bias[...]).astype(rows.dtype)
+    give = pltpu.make_async_copy(rows, out_hbm, sem.at[1])
+    give.start()
+    give.wait()
+    keep.wait()
 
 
 def fits(n, tokens, query_weight, mixout_weight, bound, depth):
@@ -680,19 +757,19 @@
         first_gain[None], first_bias[None], router_weight.T, branch_vector.reshape(-1, 128),
         dense_gate_weight.T, dense_up_weight.T, dense_down_weight,
         expert_gate_weight, expert_up_weight, expert_down_weight,
-        second_gain[None], second_bias[None], routes.T,
+        routes.T,
     )
     (
         _, state, query, *_, bound, head, mix, gain1, bias1, router, branch,
-        dgate, dup, ddown, gate, up, down, gain2, bias2, route,
+        dgate, dup, ddown, gate, up, down, route,
     ) = operands
     vmem = lambda a: pltpu.VMEM(a.shape, a.dtype)
     sems = lambda *shape: pltpu.SemaphoreType.DMA(shape)
-    pairs = 5 + half // 16 + chunks
-    output, fresh = pl.pallas_call(
+    one = pltpu.SemaphoreType.DMA
+    mixture, fresh = pl.pallas_call(
         functools.partial(layer_kernel, n, chunks),
         out_shape=(
-            jax.ShapeDtypeStruct((nseq, width), bf16),
+            jax.ShapeDtypeStruct((nseq, width), f32),
             jax.ShapeDtypeStruct(state.shape, f32),
         ),
         in_specs=[pl.BlockSpec(memory_space=pltpu.HBM)] * len(operands),
@@ -700,12 +777,13 @@
         scratch_shapes=[
             vmem(state), pltpu.VMEM((8 * own, width), bf16),
             pltpu.VMEM((2 * mix_own, mix.shape[1]), bf16),
-            *[vmem(a) for a in (gate, up, down, dgate, dup, ddown)],
-            *[vmem(a) for a in (bound, head, gain1, bias1, router, branch, gain2, bias2, route)],
+            pltpu.VMEM((2, *gate.shape), bf16), vmem(down), pltpu.VMEM((2, *dgate.shape), bf16), vmem(ddown),
+            *[vmem(a) for a in (bound, head, gain1, bias1, router, branch, route)],
             pltpu.VMEM((chips, nseq, width), bf16), pltpu.VMEM((half, width), bf16),
             pltpu.VMEM((chips, nseq, 8 * own), bf16), pltpu.VMEM((chips, nseq, 8 * own), bf16),
             pltpu.VMEM((chips, nseq, mix.shape[1]), bf16), pltpu.VMEM((half, mix.shape[1]), bf16),
-            pltpu.VMEM((chips, half, 2 * mix_own), bf16), pltpu.VMEM((2 * half, width), bf16),
+            pltpu.VMEM((chips, half, 2 * mix_own), bf16), pltpu.VMEM((half, width), f32),
+            pltpu.VMEM((2 * half, width), bf16),
             pltpu.VMEM((heads * nseq // 4, 2 * depth, 2 * depth), bf16),
             pltpu.VMEM((heads * nseq // 4, 2 * depth, 2 * depth), bf16),
             pltpu.VMEM((16, width), bf16),
@@ -715,14 +793,27 @@
             pltpu.VMEM((chunks, half, width // chunks), bf16),
             pltpu.VMEM((chunks, chips, nseq, width // chunks), bf16),
             pltpu.VMEM((chunks, chips, nseq, width // chunks), bf16),
-            sems(len(operands)),
-            *[sems(chips)] * 8, sems(chunks, chips), sems(chunks, chips), sems(pairs), sems(pairs),
+            pltpu.SemaphoreType.REGULAR((PLANE - 1 + chips // PLANE - 1,)), sems(15),
+            one, sems(chips // PLANE), one, one, one, one, one, sems(chips // PLANE),
+            sems(chunks), sems(chunks), sems(3 + chunks), sems(3 + chunks),
         ],
         compiler_params=pltpu.CompilerParams(
             collective_id=3, has_side_effects=True, vmem_limit_bytes=44 * 2**20
         ),
-    )(*operands)
-    return output, fresh.reshape(recurrent_state.shape)
+    )(*[pltpu.with_memory_space_constraint(a, pltpu.HBM) for a in operands])
+    anywhere, here = pl.BlockSpec(memory_space=pl.ANY), pl.BlockSpec(memory_space=pltpu.VMEM)
+    output, new_state = pl.pallas_call(
+        finish_kernel,
+        out_shape=(
+            jax.ShapeDtypeStruct((nseq, width), bf16),
+            jax.ShapeDtypeStruct(state.shape, f32),
+        ),
+        in_specs=[here] * 4,
+        out_specs=(anywhere, anywhere),
+        scratch_shapes=[pltpu.VMEM((nseq, width), bf16), sems(2)],
+        compiler_params=pltpu.CompilerParams(vmem_limit_bytes=4 * 2**20),
+    )(mixture, fresh, second_gain[None], second_bias[None])
+    return output, new_state.reshape(recurrent_state.shape)
 
 
 def per_device(

time: 71.1 us -> 48.5 us (0.68)
  local copies, waits for them, and re-layouts: 18.3 us -> 0.01 us
  Pallas kernels: 51.3 us -> 47.7 us
    unnamed x40 -> x4, local copies, waits for them, and re-layouts: 18.3 us -> 0.01 us
    pallas_call x1, Pallas kernels: 51.3 us -> 46.3 us  [whole_layer(): pl.pallas_call(functools.partial(layer_kernel, n, chunks), out_shape=(jax...]
    pallas_call x0 -> x1, Pallas kernels: none -> 1.34 us  [whole_layer(): pl.pallas_call(finish_kernel, out_shape=(jax.ShapeDtypeStruct((nseq, widt...]
where the time goes in v2:
time: 48.5 us; the launch traced here: 48.4 us
  Pallas kernels  47.7 us (98%)
  between operations  0.68 us (1%)
    pallas_call x1, Pallas kernels, whole_layer(): pl.pallas_call(functools.partial(layer_kernel, n, chunks), out_shape=(jax...  46.3 us
    pallas_call x1, Pallas kernels, whole_layer(): pl.pallas_call(finish_kernel, out_shape=(jax.ShapeDtypeStruct((nseq, widt...  1.34 us

profile of v2, /device:TPU:0, one launch (start us, length us, event | category | flops | bytes accessed | tf_op | source)
XLA Modules:
  0.0 48.4 jit_solution(14287233350231553548)
XLA Ops:
  0.6 0.0 copy-start
  0.6 0.0 copy-start.1
  0.7 46.3 %shard_map.221 = (f32[4,2048]{1,0:T(4,128)S(1)}, f32[32,128,128]{2,1,0:T(8,128)S(1)}) custom-call(bf16[4,2048]{1,0:T(4,128)(2,1)} %tokens_hbm.1, f32[32,128,128]{2,1,0:T(8,128)} %bitcast.20, bf16[32,2048]{1,0:T(8,128)(2,1)} %bitcast.23, bf16[32,2048]{1,0:T(8,128)(2,1)} %bitcast.24, bf16[32,2048]{1,0:T(8,128)(2,1)} %bitcast.25, bf16[32,2048]{1,0:T(8,128)(2,1)} %bitcast.26, ...), custom_call_target="tpu_custom_call" | custom-call | tf_op jit(solution)/shard_map/pallas_call | solution.py:769
  47.0 0.0 copy-done
  47.0 0.0 copy-done.1
  47.0 1.3 %shard_map.222 = (bf16[4,2048]{1,0:T(4,128)(2,1)}, f32[32,128,128]{2,1,0:T(8,128)}) custom-call(f32[4,2048]{1,0:T(4,128)S(1)} %get-tuple-element.6.mixture, f32[32,128,128]{2,1,0:T(8,128)S(1)} %get-tuple-element.7.fresh, f32[1,2048]{1,0:T(1,128)S(1)} %bitcast.18, f32[1,2048]{1,0:T(1,128)S(1)} %bitcast.19), custom_call_target="tpu_custom_call" | custom-call | tf_op jit(solution)/shard_map/pallas_call | solution.py:805
Async XLA Ops:
  0.6 46.4 %copy-start = (f32[2048]{0:T(1024)S(1)}, f32[2048]{0:T(1024)}, u32[]{:S(2)}) copy-start(f32[2048]{0:T(1024)} %param.41) | copy-start | bytes 24580
  0.6 46.4 %copy-start.1 = (f32[2048]{0:T(1024)S(1)}, f32[2048]{0:T(1024)}, u32[]{:S(2)}) copy-start(f32[2048]{0:T(1024)} %param.42) | copy-start | bytes 24580
